TPU v7x, 32 devices: a whole 2x2x4 slice. The times are simulated.
32 devices in a mesh: ep: 8 (over z, y), tp: 4 (over x, core).
Axes of the slice: x: 2, y: 2, z: 4, core: 2. Of those that a mesh axis runs over, the one named last changes fastest.
Arguments:
- tokens: bfloat16 [192, 1024], P('ep'), may hold values from -6 to 6
- mixer_gain: float32 [1024], replicated, may hold values from 0.1 to 1.9
- gate_weight: bfloat16 [1024, 1024], P(None, 'tp'), may hold values from -0.1875 to 0.1875
- inner_weight: bfloat16 [1024, 1024], P(None, 'tp'), may hold values from -0.1875 to 0.1875
- state_weight: bfloat16 [2, 1024, 512], P(None, None, 'tp'), may hold values from -0.1875 to 0.1875
- step_weight: bfloat16 [1024, 16], P(None, 'tp'), may hold values from -0.1875 to 0.1875
- step_bias: float32 [16], P('tp'), may hold values from -4 to 0.5
- decay_log: float32 [16], P('tp'), may hold values from 0 to 2.8
- skip_scale: float32 [16], P('tp'), may hold values from 0.5 to 1.5
- inner_kernel: float32 [4, 1024], P(None, 'tp'), may hold values from -3 to 3
- state_kernel: float32 [4, 2, 512], P(None, None, 'tp'), may hold values from -3 to 3
- inner_window: bfloat16 [192, 3, 1024], P('ep', None, 'tp'), may hold values from -6 to 6
- state_window: bfloat16 [192, 3, 2, 512], P('ep', None, None, 'tp'), may hold values from -6 to 6
- recurrent_state: float32 [192, 16, 64, 128], P('ep', 'tp'), may hold values from -2.4 to 2.4
- group_gain: float32 [1024], P('tp'), may hold values from 0.1 to 1.9
- output_weight: bfloat16 [1024, 1024], P('tp'), may hold values from -0.1875 to 0.1875
- channel_gain: float32 [1024], replicated, may hold values from 0.1 to 1.9
- routes: int32 [192, 2], P('ep'), may hold values from 0 to 7, all different within a row; in each aligned block of 24 rows (0 to 23, 24 to 47, ...) at most 9 rows name the same one
- route_weights: float32 [192, 2], P('ep'), may hold values from 0.2 to 1
- expert_gate: bfloat16 [8, 1024, 2816], P('ep', None, 'tp'), may hold values from -0.1875 to 0.1875
- expert_up: bfloat16 [8, 1024, 2816], P('ep', None, 'tp'), may hold values from -0.1875 to 0.1875
- expert_down: bfloat16 [8, 2816, 1024], P('ep', 'tp'), may hold values from -0.109375 to 0.109375
- dense_gate: bfloat16 [1024, 2816], P('tp', 'ep'), may hold values from -0.1875 to 0.1875
- dense_up: bfloat16 [1024, 2816], P('tp', 'ep'), may hold values from -0.1875 to 0.1875
- dense_down: bfloat16 [2816, 1024], P('ep', 'tp'), may hold values from -0.109375 to 0.109375
- dense_scale: float32 [1024], P('tp'), may hold values from 0.3 to 1.5
Outputs:
- new_tokens: bfloat16 [192, 1024], P('ep', 'tp')
- new_state: float32 [192, 16, 64, 128], P('ep', 'tp')
- new_inner_window: bfloat16 [192, 3, 1024], P('ep', None, 'tp')
- new_state_window: bfloat16 [192, 3, 2, 512], P('ep', None, None, 'tp')
Inputs may be any that keep to these rules, and one draw needn't show every extreme that they name: `routes`: each row names 2 different experts. Within the rows of one device (aligned blocks of 24 rows) no expert is named by more than 9 rows, and in some block an expert is named by exactly 9 rows.
All inputs are finite; a program needn't handle non-finite values.
Results may differ from a plain program's by a relative error of at most 0.014.
Values may be sent and summed in bfloat16 or wider, within the bound.
A program may use at most 64 MiB of HBM per device.

v0:
```python
import jax
import jax.numpy as jnp
from jax import lax
from jax.sharding import PartitionSpec as P

HEADS = 16
GROUPS = 4
HEAD_DIM = 64
STATE_DIM = 128


eps = 1e-06


def rms_scale(values, norm_gain):
    squares = jnp.mean(values * values, axis=-1, keepdims=True)
    return values * lax.rsqrt(squares + eps) * norm_gain


def local(
    tokens,
    mixer_gain,
    gate_weight,
    inner_weight,
    state_weight,
    step_weight,
    step_bias,
    decay_log,
    skip_scale,
    inner_kernel,
    state_kernel,
    inner_window,
    state_window,
    recurrent_state,
    group_gain,
    output_weight,
    channel_gain,
    routes,
    route_weights,
    expert_gate,
    expert_up,
    expert_down,
    dense_gate,
    dense_up,
    dense_down,
    dense_scale,
):
    f32 = jnp.float32
    bf16 = jnp.bfloat16
    seq_count = tokens.shape[0]
    residual = tokens.astype(f32)
    normed = rms_scale(residual, mixer_gain).astype(bf16)
    gate_pre = jnp.dot(normed, gate_weight, preferred_element_type=f32)
    inner_pre = jnp.dot(normed, inner_weight, preferred_element_type=f32).astype(bf16)
    state_pre = jnp.stack(
        [
            jnp.dot(normed, state_weight[0], preferred_element_type=f32),
            jnp.dot(normed, state_weight[1], preferred_element_type=f32),
        ],
        axis=1,
    ).astype(bf16)
    step_raw = jnp.dot(normed, step_weight, preferred_element_type=f32)
    inner_ctx = jnp.concatenate([inner_window, inner_pre[:, None, :]], axis=1)
    inner_conv = jax.nn.silu(jnp.sum(inner_ctx.astype(f32) * inner_kernel[None], axis=1))
    state_ctx = jnp.concatenate([state_window, state_pre[:, None]], axis=1)
    state_conv = jax.nn.silu(jnp.sum(state_ctx.astype(f32) * state_kernel[None], axis=1))
    per_group = HEADS // GROUPS
    local_groups = state_conv.shape[-1] // STATE_DIM
    step_size = jax.nn.softplus(step_raw + step_bias)
    decay_rate = jnp.exp(-step_size * jnp.exp(decay_log))
    shaped = (seq_count, local_groups, per_group)
    inner_heads = inner_conv.reshape(seq_count, local_groups, per_group, HEAD_DIM)
    in_vector = state_conv[:, 0].reshape(seq_count, local_groups, STATE_DIM)
    out_vector = state_conv[:, 1].reshape(seq_count, local_groups, STATE_DIM)
    old_state = recurrent_state.reshape(seq_count, local_groups, per_group, HEAD_DIM, STATE_DIM)
    written = (step_size.reshape(shaped)[..., None] * inner_heads)[..., None] * in_vector[
        :, :, None, None, :
    ]
    new_state = old_state * decay_rate.reshape(shaped)[..., None, None] + written
    mixed_out = jnp.einsum(
        "sgrpn,sgn->sgrp", new_state, out_vector, precision=lax.Precision.HIGHEST
    )
    mixed_out = (
        mixed_out + skip_scale.reshape(local_groups, per_group)[None, :, :, None] * inner_heads
    )
    gated_out = mixed_out.reshape(seq_count, -1) * jax.nn.silu(gate_pre)
    grouped = rms_scale(gated_out.reshape(seq_count, local_groups, -1), 1.0).reshape(seq_count, -1)
    mixer_rows = (grouped * group_gain).astype(bf16)
    partial_value = jnp.dot(mixer_rows, output_weight, preferred_element_type=f32)
    residual = residual + lax.psum(partial_value.astype(jnp.bfloat16), "tp").astype(jnp.float32)
    ffn_rows = rms_scale(residual, channel_gain).astype(bf16)
    local_width = dense_gate.shape[0]
    tp_index = lax.axis_index("tp")
    own_columns = lax.dynamic_slice_in_dim(ffn_rows, tp_index * local_width, local_width, 1)
    residual_columns = lax.dynamic_slice_in_dim(residual, tp_index * local_width, local_width, 1)
    gate_whole, up_whole, down_whole = (
        lax.all_gather(dense_gate, "ep", axis=1, tiled=True),
        lax.all_gather(dense_up, "ep", axis=1, tiled=True),
        lax.all_gather(dense_down, "ep", axis=0, tiled=True),
    )
    gate_up = jnp.stack(
        [
            jnp.dot(own_columns, gate_whole, preferred_element_type=f32),
            jnp.dot(own_columns, up_whole, preferred_element_type=f32),
        ],
        axis=0,
    )
    gate_up = lax.psum(gate_up.astype(jnp.bfloat16), "tp").astype(jnp.float32)
    hidden_rows = (jax.nn.silu(gate_up[0]) * gate_up[1]).astype(bf16)
    dense_out = jnp.dot(hidden_rows, down_whole, preferred_element_type=f32)
    topk_count = routes.shape[1]
    local_experts = expert_gate.shape[0]
    expert_count = local_experts * lax.axis_size("ep")
    capacity = max(2, seq_count * topk_count * 3 // (2 * expert_count))
    flat_routes = routes.reshape(-1)
    onehot = (flat_routes[:, None] == jnp.arange(expert_count, dtype=jnp.int32)[None, :]).astype(
        jnp.int32
    )
    rank_before = jnp.cumsum(onehot, axis=0) - onehot
    slot_index = jnp.sum(rank_before * onehot, axis=1)
    target = flat_routes * capacity + slot_index
    placing = jnp.arange(expert_count * capacity, dtype=jnp.int32)[:, None] == target[None, :]
    selection = jnp.any(
        placing.reshape(expert_count * capacity, seq_count, topk_count), axis=2
    ).astype(bf16)
    outgoing = jnp.dot(selection, ffn_rows, preferred_element_type=f32).astype(bf16)
    outgoing = outgoing.reshape(expert_count, capacity, -1)
    arrived = lax.all_to_all(outgoing, "ep", split_axis=0, concat_axis=0, tiled=True)
    sources = arrived.shape[0] // local_experts
    items = arrived.shape[1]
    grouped_in = arrived.reshape(sources, local_experts, items, arrived.shape[2])
    gate_act = jnp.einsum("seid,edf->seif", grouped_in, expert_gate, preferred_element_type=f32)
    up_act = jnp.einsum("seid,edf->seif", grouped_in, expert_up, preferred_element_type=f32)
    activated = (jax.nn.silu(gate_act) * up_act).astype(bf16)
    partial_out = jnp.einsum("seif,efd->seid", activated, expert_down, preferred_element_type=f32)
    partial_out = partial_out.reshape(arrived.shape[0], items, -1)
    processed = (
        lax.psum_scatter(partial_out.astype(jnp.bfloat16), "tp", scatter_dimension=2, tiled=True)
        .astype(jnp.float32)
        .astype(bf16)
    )
    returned = lax.all_to_all(processed, "ep", split_axis=0, concat_axis=0, tiled=True)
    returned_rows = returned.reshape(expert_count * capacity, -1)
    picked = jnp.einsum(
        "ms,md->sd", placing.astype(bf16), returned_rows, preferred_element_type=f32
    )
    expert_out = jnp.sum(
        picked.reshape(seq_count, topk_count, -1) * route_weights[:, :, None], axis=1
    )
    new_tokens = (residual_columns + expert_out + dense_scale * dense_out).astype(bf16)
    return (
        new_tokens,
        new_state.reshape(seq_count, -1, HEAD_DIM, STATE_DIM),
        inner_ctx[:, 1:],
        state_ctx[:, 1:],
    )


def solution(mesh):
    placed = (
        P("ep", None),
        P(),
        P(None, "tp"),
        P(None, "tp"),
        P(None, None, "tp"),
        P(None, "tp"),
        P("tp"),
        P("tp"),
        P("tp"),
        P(None, "tp"),
        P(None, None, "tp"),
        P("ep", None, "tp"),
        P("ep", None, None, "tp"),
        P("ep", "tp", None, None),
        P("tp"),
        P("tp", None),
        P(),
        P("ep", None),
        P("ep", None),
        P("ep", None, "tp"),
        P("ep", None, "tp"),
        P("ep", "tp", None),
        P("tp", "ep"),
        P("tp", "ep"),
        P("ep", "tp"),
        P("tp"),
    )
    return jax.shard_map(
        local,
        mesh=mesh,
        in_specs=placed,
        out_specs=(
            P("ep", "tp"),
            P("ep", "tp", None, None),
            P("ep", None, "tp"),
            P("ep", None, None, "tp"),
        ),
        check_vma=False,
    )
```

profile of v0, /device:TPU:1, one launch (start us, length us, event | category | flops | bytes accessed | tf_op | source)
XLA Modules:
  0.0 157.4 jit_solution(13215991995237395833)
XLA Ops:
  8.2 0.7 all-gather.4.cloned.1.call-update
  8.9 0.7 all-gather.6.cloned.1.call-update
  9.6 0.9 fusion.48
  10.5 1.2 fusion.30
  11.7 1.2 fusion.31
  13.0 1.3 fusion.29
  14.3 0.1 reduce_sum.69
  14.5 0.2 multiply_exponential_fusion
  14.7 0.1 copy.59
  15.0 0.1 copy.58
  15.1 0.1 broadcast_multiply_fusion
  15.2 2.6 %multiply_add_fusion = f32[24,4,64,128]{3,2,1,0:T(8,128)S(1)} fusion(f32[24,4,64,128]{3,2,1,0:T(8,128)} %param.39, f32[24,128]{1,0:T(8,128)S(1)} %bitcast.102, f32[24,4,64]{2,1,0:T(4,128)S(1)} %broadcast_multiply_fusion, f32[24,4]{1,0:T(8,128)S(1)} %copy.58), kind=kLoop, calls=%fused_computation.4 | loop fusion | flops 2359296 | bytes 6328704 | tf_op jit(solution)/shard_map/add | solution.py:79
  17.8 7.4 %fusion.55 = f32[24,1,4,64]{3,1,2,0:T(1,128)S(1)} fusion(f32[24,4,64,128]{3,2,1,0:T(8,128)S(1)} %multiply_add_fusion, f32[24,2,128]{2,1,0:T(2,128)S(1)} %divide_multiply_fusion.1), kind=kOutput, calls=%fused_computation.76 | convolution fusion | flops 9437184 | bytes 3182592 | tf_op jit(solution)/shard_map/sgrpn,sgn->sgrp/dot_general | solution.py:80
  25.2 0.1 multiply_add_fusion.1
  25.3 0.1 reshape.212
  25.4 0.1 copy.61
  25.5 0.1 reshape.213
  25.8 0.4 copy-done.9
  26.2 0.7 select_reduce_fusion
  26.9 0.9 reduce_sum.73
  27.7 0.6 copy.62
  28.4 1.1 multiply_reduce_fusion.3
  29.5 1.3 convolution_convert_fusion.3
  30.7 11.8 %psum.14 = bf16[24,1024]{1,0:T(8,128)(2,1)S(1)} all-reduce(bf16[24,1024]{1,0:T(8,128)(2,1)S(1)} %convolution_convert_fusion.3), channel_id=1, replica_groups=mesh['ep'=8,'tp'=4] {'tp'}, use_global_device_ids=true, to_apply=%region_4.5 | all-reduce | flops 24576 | bytes 98304 | tf_op jit(solution)/shard_map/psum | solution.py:90
  42.5 0.7 multiply_add_fusion.2
  43.2 0.1 fusion.53
  43.3 0.1 convert_add_fusion
  43.4 0.1 multiply_convert_fusion
  43.5 0.2 convolution_convert_fusion.2
  43.8 0.8 reshape.214
  44.6 5.7 %all-to-all-start = ((bf16[8,9,1024]{2,1,0:T(8,128)(2,1)}), bf16[8,9,1024]{2,1,0:T(8,128)(2,1)S(1)}, u32[]{:S(2)}, u32[]{:S(2)}) async-start(bf16[8,9,1024]{2,1,0:T(8,128)(2,1)} %reshape.214), calls=%async_computation | async-start | bytes 524288 | tf_op jit(solution)/shard_map/all_to_all | solution.py:128
  50.3 10.6 %all-to-all-done = bf16[8,9,1024]{2,1,0:T(8,128)(2,1)S(1)} async-done(((bf16[8,9,1024]{2,1,0:T(8,128)(2,1)}), bf16[8,9,1024]{2,1,0:T(8,128)(2,1)S(1)}, u32[]{:S(2)}, u32[]{:S(2)}) %all-to-all-start) | async-done | bytes 147488 | tf_op jit(solution)/shard_map/all_to_all | solution.py:128
  61.0 1.4 fusion.8
  62.3 3.2 %fusion.14 = bf16[8,9,1024]{2,1,0:T(8,128)(2,1)} fusion(bf16[1,704,1024]{2,1,0:T(8,128)(2,1)S(1)} %copy-done, bf16[8,9,1024]{2,1,0:T(8,128)(2,1)S(1)} %all-to-all-done, bf16[1,1024,704]{1,2,0:T(8,128)(2,1)} %param.46, f32[8,1,9,704]{3,2,0,1:T(8,128)} %fusion.8), kind=kOutput, calls=%fused_computation.13 | convolution fusion | flops 207995904 | bytes 3381248 | tf_op jit(solution)/shard_map/seif,efd->seid/dot_general | solution.py:135
  65.6 1.9 %fusion = bf16[1,24,2816]{2,1,0:T(8,128)(2,1)S(1)} fusion(bf16[256,2816]{0,1:T(8,128)(2,1)} %all-gather.4.cloned.1.call-done, bf16[24,1024]{1,0:T(8,128)(2,1)S(1)} %multiply_convert_fusion, s32[]{:T(128)S(6)} %select_n.9), kind=kOutput, calls=%fused_computation.2 | convolution fusion | flops 34670592 | bytes 1589252 | tf_op jit(solution)/shard_map/dot_general | solution.py:103
  67.5 33.5 %all-gather.6.cloned.1.call-done = bf16[256,2816]{0,1:T(8,128)(2,1)} async-done(((bf16[256,352]{0,1:T(8,128)(2,1)}), bf16[256,2816]{0,1:T(8,128)(2,1)}) %all-gather.6.cloned.1.call-update) | async-done | bytes 1441808 | tf_op jit(solution)/shard_map/all_gather | solution.py:98
  101.0 1.9 %fusion.1 = bf16[1,24,2816]{2,1,0:T(8,128)(2,1)S(1)} fusion(bf16[256,2816]{0,1:T(8,128)(2,1)} %all-gather.6.cloned.1.call-done, bf16[24,1024]{1,0:T(8,128)(2,1)S(1)} %multiply_convert_fusion, s32[]{:T(128)S(6)} %select_n.9), kind=kOutput, calls=%fused_computation.3 | convolution fusion | flops 34670592 | bytes 1589252 | tf_op jit(solution)/shard_map/dot_general | solution.py:104
  102.9 0.7 pad_maximum_fusion
  103.7 0.7 all-gather.8.cloned.1.call-update
  104.4 0.6 slice.38
  105.2 3.4 %all-to-all-start.1 = ((bf16[8,9,256]{2,1,0:T(8,128)(2,1)}), bf16[8,9,256]{2,1,0:T(8,128)(2,1)S(1)}, u32[]{:S(2)}, u32[]{:S(2)}) async-start(bf16[8,9,256]{2,1,0:T(8,128)(2,1)} %reduce-scatter.2.cloned.1.call-done), calls=%async_computation.2 | async-start | bytes 131072 | tf_op jit(solution)/shard_map/all_to_all | solution.py:142
  108.5 0.6 fusion.51
  109.2 5.2 %all-to-all-done.1 = bf16[8,9,256]{2,1,0:T(8,128)(2,1)S(1)} async-done(((bf16[8,9,256]{2,1,0:T(8,128)(2,1)}), bf16[8,9,256]{2,1,0:T(8,128)(2,1)S(1)}, u32[]{:S(2)}, u32[]{:S(2)}) %all-to-all-start.1) | async-done | bytes 36896 | tf_op jit(solution)/shard_map/all_to_all | solution.py:142
  114.4 0.1 fusion.26
  114.4 19.5 %all-reduce.2.cloned.1.call-done = bf16[2,24,2816]{2,1,0:T(8,128)(2,1)} async-done(((bf16[2,24,2816]{2,1,0:T(8,128)(2,1)}), bf16[2,24,2816]{2,1,0:T(8,128)(2,1)}) %all-reduce.2.cloned.1.call-update) | async-done | bytes 270352 | tf_op jit(solution)/shard_map/psum | solution.py:108
  133.9 1.0 convert_element_type.74
  134.9 13.1 %all-gather.8.cloned.1.call-done = bf16[2816,256]{1,0:T(8,128)(2,1)} async-done(((bf16[352,256]{1,0:T(8,128)(2,1)}), bf16[2816,256]{1,0:T(8,128)(2,1)}) %all-gather.8.cloned.1.call-update) | async-done | bytes 1441808 | tf_op jit(solution)/shard_map/all_gather | solution.py:99
  148.0 2.3 %fusion.28 = bf16[24,256]{1,0:T(8,128)(2,1)} fusion(bf16[2816,256]{1,0:T(8,128)(2,1)} %all-gather.8.cloned.1.call-done, f32[2,24,2816]{2,1,0:T(8,128)S(1)} %convert_element_type.74, f32[24,256]{1,0:T(8,128)S(1)} %fusion.26, f32[24,1024]{1,0:T(8,128)S(1)} %get-tuple-element.4, s32[]{:T(128)S(6)} %select_n.9, f32[256]{0:T(256)S(1)} %copy-done.20), kind=kOutput, calls=%fused_computation.23 | convolution fusion | flops 35033088 | bytes 2044932 | tf_op jit(solution)/shard_map/dot_general | solution.py:110
  (71 shorter events, 0.9 us)
Async XLA Ops:
  8.0 54.3 %copy-start = (bf16[1,704,1024]{2,1,0:T(8,128)(2,1)S(1)}, bf16[1,704,1024]{2,1,0:T(8,128)(2,1)}, u32[]{:S(2)}) copy-start(bf16[1,704,1024]{2,1,0:T(8,128)(2,1)} %param.47) | copy-start | bytes 4325380
  8.0 6.4 %copy-start.3 = (bf16[24,1024]{1,0:T(8,128)(2,1)S(1)}, bf16[24,1024]{1,0:T(8,128)(2,1)}, u32[]{:S(2)}) copy-start(bf16[24,1024]{1,0:T(8,128)(2,1)} %param.26) | copy-start | bytes 147460
  8.0 6.4 %copy-start.8 = (f32[1024]{0:T(1024)S(1)}, f32[1024]{0:T(1024)}, u32[]{:S(2)}) copy-start(f32[1024]{0:T(1024)} %param.27) | copy-start | bytes 12292
  8.0 6.2 %copy-start.11 = (f32[4,256]{1,0:T(4,128)S(1)}, f32[4,256]{1,0:T(4,128)}, u32[]{:S(2)}) copy-start(f32[4,256]{1,0:T(4,128)} %param.35) | copy-start | bytes 12292
  8.0 6.2 %copy-start.5 = (bf16[24,3,256]{2,0,1:T(8,128)(2,1)S(1)}, bf16[24,3,256]{2,0,1:T(8,128)(2,1)}, u32[]{:S(2)}) copy-start(bf16[24,3,256]{2,0,1:T(8,128)(2,1)} %param.37) | copy-start | bytes 110596
  8.1 6.3 %copy-start.21 = (f32[4]{0:T(128)S(1)}, f32[4]{0:T(128)}, u32[]{:S(2)}) copy-start(f32[4]{0:T(128)} %param.33) | copy-start | bytes 52
  8.1 6.4 %copy-start.18 = (bf16[1024,4]{0,1:T(4,128)(2,1)S(1)}, bf16[1024,4]{0,1:T(4,128)(2,1)}, u32[]{:S(2)}) copy-start(bf16[1024,4]{0,1:T(4,128)(2,1)} %param.31) | copy-start | bytes 24580
  8.1 6.4 %copy-start.22 = (f32[4]{0:T(128)S(1)}, f32[4]{0:T(128)}, u32[]{:S(2)}) copy-start(f32[4]{0:T(128)} %param.32) | copy-start | bytes 52
  8.1 6.7 %copy-start.7 = (bf16[24,3,2,128]{3,2,1,0:T(2,128)(2,1)S(1)}, bf16[24,3,2,128]{3,2,1,0:T(2,128)(2,1)}, u32[]{:S(2)}) copy-start(bf16[24,3,2,128]{3,2,1,0:T(2,128)(2,1)} %param.38) | copy-start | bytes 110596
  8.1 6.8 %copy-start.12 = (f32[4,2,128]{2,1,0:T(2,128)S(1)}, f32[4,2,128]{2,1,0:T(2,128)}, u32[]{:S(2)}) copy-start(f32[4,2,128]{2,1,0:T(2,128)} %param.36) | copy-start | bytes 12292
  8.1 57.5 %all-gather.4.cloned.1.call-start = ((), (), s32[]{:S(2)}) async-start(), calls=%async_computation.4 | async-start | bytes 1622016 | tf_op jit(solution)/shard_map/all_gather | solution.py:97
  8.8 92.2 %all-gather.6.cloned.1.call-start = ((), (), s32[]{:S(2)}) async-start(), calls=%async_computation.5 | async-start | bytes 1622016 | tf_op jit(solution)/shard_map/all_gather | solution.py:98
  10.5 4.2 %copy-start.16 = (f32[24]{0:T(128)}, f32[24]{0:T(128)S(1)}, u32[]{:S(2)}) copy-start(f32[24]{0:T(128)S(1)} %add_rsqrt_fusion.2) | copy-start | bytes 292
  17.8 7.4 %copy-start.1 = (f32[24,4,64,128]{3,2,1,0:T(8,128)}, f32[24,4,64,128]{3,2,1,0:T(8,128)S(1)}, u32[]{:S(2)}) copy-start(f32[24,4,64,128]{3,2,1,0:T(8,128)S(1)} %multiply_add_fusion) | copy-start | bytes 9437188
  17.8 7.4 %copy-start.17 = (f32[4]{0:T(128)S(1)}, f32[4]{0:T(128)}, u32[]{:S(2)}) copy-start(f32[4]{0:T(128)} %param.34) | copy-start | bytes 52
  17.8 7.6 %copy-start.14 = (s32[24,2]{0,1:T(2,128)S(1)}, s32[24,2]{0,1:T(2,128)}, u32[]{:S(2)}) copy-start(s32[24,2]{0,1:T(2,128)} %param.43) | copy-start | bytes 580
  17.8 10.6 %copy-start.4 = (bf16[1024,256]{1,0:T(8,128)(2,1)S(1)}, bf16[1024,256]{1,0:T(8,128)(2,1)}, u32[]{:S(2)}) copy-start(bf16[1024,256]{1,0:T(8,128)(2,1)} %param.28) | copy-start | bytes 1572868
  25.6 0.6 copy-start.9
  26.9 34.1 %copy-start.2 = (bf16[1,1024,704]{1,2,0:T(8,128)(2,1)S(1)}, bf16[1,1024,704]{1,2,0:T(8,128)(2,1)}, u32[]{:S(2)}) copy-start(bf16[1,1024,704]{1,2,0:T(8,128)(2,1)} %param.45) | copy-start | bytes 4325380
  28.4 15.1 %copy-start.13 = (f32[1024]{0:T(1024)S(1)}, f32[1024]{0:T(1024)}, u32[]{:S(2)}) copy-start(f32[1024]{0:T(1024)} %param.42) | copy-start | bytes 12292
  44.6 16.4 %all-to-all-start = ((bf16[8,9,1024]{2,1,0:T(8,128)(2,1)}), bf16[8,9,1024]{2,1,0:T(8,128)(2,1)S(1)}, u32[]{:S(2)}, u32[]{:S(2)}) async-start(bf16[8,9,1024]{2,1,0:T(8,128)(2,1)} %reshape.214), calls=%async_computation | async-start | bytes 524288 | tf_op jit(solution)/shard_map/all_to_all | solution.py:128
  50.3 54.9 %reduce-scatter.2.cloned.1.call-start = ((), (), s32[]{:S(2)}) async-start(), calls=%async_computation.3 | async-start | bytes 327680 | tf_op jit(solution)/shard_map/reduce_scatter | solution.py:138
  65.5 68.4 %all-reduce.2.cloned.1.call-start = ((), (), s32[]{:S(2)}) async-start(), calls=%async_computation.6 | async-start | bytes 540672 | tf_op jit(solution)/shard_map/psum | solution.py:108
  67.5 37.5 %copy-start.10 = (s32[48]{0:T(128)S(1)}, s32[48]{0:T(128)}, u32[]{:S(2)}) copy-start(s32[48]{0:T(128)} %copy-done.9) | copy-start | bytes 580
  67.5 37.5 %copy-start.15 = (s32[48]{0:T(128)S(1)}, s32[48]{0:T(128)}, u32[]{:S(2)}) copy-start(s32[48]{0:T(128)} %select_reduce_fusion) | copy-start | bytes 580
  67.5 41.0 %copy-start.6 = (bf16[24,3,256]{2,0,1:T(8,128)(2,1)S(1)}, bf16[24,3,256]{2,0,1:T(8,128)(2,1)}, u32[]{:S(2)}) copy-start(bf16[24,3,256]{2,0,1:T(8,128)(2,1)} %param.37) | copy-start | bytes 110596
  67.5 46.8 %copy-start.19 = (f32[24,2]{0,1:T(2,128)S(1)}, f32[24,2]{0,1:T(2,128)}, u32[]{:S(2)}) copy-start(f32[24,2]{0,1:T(2,128)} %param.44) | copy-start | bytes 580
  102.9 45.1 %copy-start.20 = (f32[256]{0:T(256)S(1)}, f32[256]{0:T(256)}, u32[]{:S(2)}) copy-start(f32[256]{0:T(256)} %param.51) | copy-start | bytes 3076
  103.6 44.3 %all-gather.8.cloned.1.call-start = ((), (), s32[]{:S(2)}) async-start(), calls=%async_computation.7 | async-start | bytes 1622016 | tf_op jit(solution)/shard_map/all_gather | solution.py:99
  105.2 9.2 %all-to-all-start.1 = ((bf16[8,9,256]{2,1,0:T(8,128)(2,1)}), bf16[8,9,256]{2,1,0:T(8,128)(2,1)S(1)}, u32[]{:S(2)}, u32[]{:S(2)}) async-start(bf16[8,9,256]{2,1,0:T(8,128)(2,1)} %reduce-scatter.2.cloned.1.call-done), calls=%async_computation.2 | async-start | bytes 131072 | tf_op jit(solution)/shard_map/all_to_all | solution.py:142
Sparse Core Ops, SparseCore 0:
  11.1 43.9 all-gather.3
  57.3 43.7 all-gather.5
  106.6 41.3 all-gather.7
Sparse Core Ops, SparseCore 1:
  65.6 18.5 reduce-scatter.1
  103.7 30.1 all-reduce.1
where the time goes:
time: 160 us; the launch traced here: 157 us
  waiting for transfers between devices  83.9 us (52%)
  matrix products  24.6 us (15%)
  between operations  15.6 us (10%)
  blocking collectives  11.8 us (7%)
  starting transfers between devices  9.28 us (6%)
  other arithmetic  8.08 us (5%)
  local copies, waits for them, and re-layouts  4.14 us (3%)
    all_gather x1, waiting for transfers between devices, local(): lax.all_gather(dense_up, 'ep', axis=1, tiled=True)  33.5 us
    psum x1, waiting for transfers between devices, local(): gate_up = lax.psum(gate_up.astype(jnp.bfloat16), 'tp').astype(jnp.float32)  19.5 us
    all_gather x1, waiting for transfers between devices, local(): lax.all_gather(dense_down, 'ep', axis=0, tiled=True)  13.1 us
    psum x1, blocking collectives, local(): lax.psum(partial_value.astype(jnp.bfloat16), 'tp').astype(jnp.float32)  11.8 us
    all_to_all x1, waiting for transfers between devices, local(): lax.all_to_all(outgoing, 'ep', split_axis=0, concat_axis=0, tiled=True)  10.6 us
    dot_general x1, matrix products, local(): jnp.einsum('sgrpn,sgn->sgrp', new_state, out_vector, precision=lax.Precis...  7.39 us
    all_to_all x1, starting transfers between devices, local(): lax.all_to_all(outgoing, 'ep', split_axis=0, concat_axis=0, tiled=True)  5.72 us
    all_to_all x1, waiting for transfers between devices, local(): lax.all_to_all(processed, 'ep', split_axis=0, concat_axis=0, tiled=True)  5.15 us
  transfers between devices with their start and end apart: 7, of which 5 were waited for; matrix products, arithmetic and copies ran while one was open for 22% of the time, Pallas kernels for 0%

commit v1 on v0

v1 whole, which is shorter than its diff:
```python
import functools

import jax
import jax.numpy as jnp
from jax import lax
from jax.experimental import pallas as pl
from jax.experimental.pallas import tpu as pltpu
from jax.sharding import PartitionSpec as P

HEADS = 16
GROUPS = 4
HEAD_DIM = 64
STATE_DIM = 128


eps = 1e-06


def rms_scale(values, norm_gain):
    squares = jnp.mean(values * values, axis=-1, keepdims=True)
    return values * lax.rsqrt(squares + eps) * norm_gain


def silu(v):
    return v / (1.0 + jnp.exp(-v))


def branches(
    ep_size,
    tp_size,
    part,
    tokens,
    gain,
    mix,
    scale,
    gate_hbm,
    up_hbm,
    down_hbm,
    dgate_hbm,
    dup_hbm,
    ddown_hbm,
    out,
    gate_w,
    up_w,
    down_w,
    dgate_w,
    dup_w,
    ddown_w,
    parts,
    mixes,
    residual,
    rows,
    flat,
    packed,
    pre_send,
    pre_recv,
    hidden,
    y_send,
    y_recv,
    z_send,
    z_recv,
    load_sem,
    part_sems,
    mix_sems,
    row_sems,
    relay_sems,
    pre_sems,
    hid_sems,
    y_sems,
    z_sems,
):
    f32 = jnp.float32
    bf16 = jnp.bfloat16
    me_e = lax.axis_index("ep")
    me_t = lax.axis_index("tp")
    half = lax.rem(me_t, 2)
    partner = me_t + 1 - 2 * half
    count, width = part.shape
    half_width = width // 2
    own_width = width // tp_size
    total = ep_size * count
    block = total // tp_size

    def remote(src, dst, sems, slot, to_e, to_t):
        return pltpu.make_async_remote_copy(
            src_ref=src,
            dst_ref=dst,
            send_sem=sems.at[0, slot],
            recv_sem=sems.at[1, slot],
            device_id=(to_e, to_t),
            device_id_type=pl.DeviceIdType.MESH,
        )

    barrier = pltpu.get_barrier_semaphore()
    for d in range(1, ep_size):
        pl.semaphore_signal(
            barrier,
            inc=1,
            device_id=(lax.rem(me_e + d, ep_size), me_t),
            device_id_type=pl.DeviceIdType.MESH,
        )
    for d in range(1, tp_size):
        pl.semaphore_signal(
            barrier,
            inc=1,
            device_id=(me_e, lax.rem(me_t + d, tp_size)),
            device_id_type=pl.DeviceIdType.MESH,
        )
    loads = []
    for i, (src, dst) in enumerate(
        [
            (dgate_hbm, dgate_w),
            (dup_hbm, dup_w),
            (gate_hbm, gate_w),
            (up_hbm, up_w),
            (down_hbm, down_w),
            (ddown_hbm, ddown_w),
        ]
    ):
        copy = pltpu.make_async_copy(src, dst, load_sem.at[i])
        copy.start()
        loads.append(copy)
    pl.semaphore_wait(barrier, ep_size + tp_size - 2)

    ep_peers = [lax.rem(me_e + d, ep_size) for d in range(ep_size)]
    tp_peers = [lax.rem(me_t + d, tp_size) for d in range(tp_size)]
    part_copies = [
        remote(part, parts.at[d], part_sems, d, me_e, tp_peers[d]) for d in range(1, tp_size)
    ]
    for copy in part_copies:
        copy.start()
    mix_copies = [
        remote(mix, mixes.at[d], mix_sems, d, ep_peers[d], me_t) for d in range(1, ep_size)
    ]
    for copy in mix_copies:
        copy.start()

    value = tokens[...].astype(f32) + part[...].astype(f32)
    for d in range(1, tp_size):
        part_copies[d - 1].wait_recv()
        value = value + parts[d].astype(f32)
    residual[...] = value
    ffn = rms_scale(value, gain[...]).astype(bf16)
    rows[0, 0] = ffn[:, :half_width]
    rows[1, 0] = ffn[:, half_width:]
    row_copies = [
        remote(rows.at[half, 0], rows.at[half, d], row_sems, d, ep_peers[d], me_t)
        for d in range(1, ep_size)
    ]
    for copy in row_copies:
        copy.start()
    relay_copies = []
    for d in range(1, ep_size):
        row_copies[d - 1].wait_recv()
        copy = remote(rows.at[half, d], rows.at[half, d], relay_sems, d, me_e, partner)
        copy.start()
        relay_copies.append(copy)
    for copy in relay_copies:
        copy.wait_recv()
    for d in range(ep_size):
        flat[d * count : (d + 1) * count, :half_width] = rows[0, d].astype(f32)
        flat[d * count : (d + 1) * count, half_width:] = rows[1, d].astype(f32)
    packed[...] = flat[...].astype(bf16)

    loads[0].wait()
    loads[1].wait()
    own = pl.ds(pl.multiple_of(me_t * own_width, own_width), own_width)
    for t in range(tp_size):
        piece = packed[t * block : (t + 1) * block, own]
        pre_send[t, 0] = jnp.dot(piece, dgate_w[...], preferred_element_type=f32).astype(bf16)
        pre_send[t, 1] = jnp.dot(piece, dup_w[...], preferred_element_type=f32).astype(bf16)
    pre_copies = [
        remote(pre_send.at[tp_peers[d]], pre_recv.at[d], pre_sems, d, me_e, tp_peers[d])
        for d in range(1, tp_size)
    ]
    for copy in pre_copies:
        copy.start()

    for d in range(1, ep_size):
        mix_copies[d - 1].wait_recv()
    mixes[0] = mix[...]
    loads[2].wait()
    loads[3].wait()
    loads[4].wait()

    chunk_blocks = 8 if ep_size % 8 == 0 else 1
    chunk = chunk_blocks * count

    def experts(step, carry):
        at = pl.ds(pl.multiple_of(step * chunk, chunk), chunk)
        x = packed[at, :]
        gate_act = jnp.dot(x, gate_w[0], preferred_element_type=f32)
        up_act = jnp.dot(x, up_w[0], preferred_element_type=f32)
        activated = (silu(gate_act) * up_act).astype(bf16)
        weights = mixes[pl.ds(step * chunk_blocks, chunk_blocks)].reshape(chunk, mix.shape[1])
        lanes = lax.broadcasted_iota(jnp.int32, weights.shape, 1)
        weight = jnp.sum(jnp.where(lanes == me_e, weights, 0.0), axis=1, keepdims=True)
        for t in range(tp_size):
            y = jnp.dot(
                activated,
                down_w[0, :, t * own_width : (t + 1) * own_width],
                preferred_element_type=f32,
            )
            y_send[t, at, :] = (y * weight).astype(bf16)
        return carry

    lax.fori_loop(0, total // chunk, experts, 0)
    y_copies = [
        remote(y_send.at[tp_peers[d]], y_recv.at[d], y_sems, d, me_e, tp_peers[d])
        for d in range(1, tp_size)
    ]

    gate_sum = pre_send[me_t, 0].astype(f32)
    up_sum = pre_send[me_t, 1].astype(f32)
    for d in range(1, tp_size):
        pre_copies[d - 1].wait_recv()
        gate_sum = gate_sum + pre_recv[d, 0].astype(f32)
        up_sum = up_sum + pre_recv[d, 1].astype(f32)
    hidden[me_t] = (silu(gate_sum) * up_sum).astype(bf16)
    hid_copies = [
        remote(hidden.at[me_t], hidden.at[me_t], hid_sems, d, me_e, tp_peers[d])
        for d in range(1, tp_size)
    ]
    for copy in hid_copies:
        copy.start()
    for copy in y_copies:
        copy.start()
    for d in range(1, tp_size):
        hid_copies[d - 1].wait_recv()
    loads[5].wait()
    for t in range(tp_size):
        dense = jnp.dot(hidden[t], ddown_w[...], preferred_element_type=f32) * scale[...]
        flat[t * block : (t + 1) * block, :own_width] = dense
    for d in range(1, tp_size):
        y_copies[d - 1].wait_recv()

    def combine(step, carry):
        at = pl.ds(pl.multiple_of(step * chunk, chunk), chunk)
        summed = flat[at, :own_width] + y_send[me_t, at, :].astype(f32)
        for d in range(1, tp_size):
            summed = summed + y_recv[d, at, :].astype(f32)
        for i in range(chunk_blocks):
            z_send[step * chunk_blocks + i] = summed[i * count : (i + 1) * count].astype(bf16)
        return carry

    lax.fori_loop(0, total // chunk, combine, 0)
    z_copies = [
        remote(
            z_send.at[d],
            z_recv.at[d],
            z_sems,
            d,
            lax.rem(me_e + ep_size - d, ep_size),
            me_t,
        )
        for d in range(1, ep_size)
    ]
    for copy in z_copies:
        copy.start()
    final = residual[:, own] + z_send[0].astype(f32)
    for d in range(1, ep_size):
        z_copies[d - 1].wait_recv()
        final = final + z_recv[d].astype(f32)
    out[...] = final.astype(bf16)
    for copy in part_copies + mix_copies + row_copies + relay_copies + pre_copies:
        copy.wait_send()
    for copy in hid_copies + y_copies + z_copies:
        copy.wait_send()


def local(
    tokens,
    mixer_gain,
    gate_weight,
    inner_weight,
    state_weight,
    step_weight,
    step_bias,
    decay_log,
    skip_scale,
    inner_kernel,
    state_kernel,
    inner_window,
    state_window,
    recurrent_state,
    group_gain,
    output_weight,
    channel_gain,
    routes,
    route_weights,
    expert_gate,
    expert_up,
    expert_down,
    dense_gate,
    dense_up,
    dense_down,
    dense_scale,
):
    f32 = jnp.float32
    bf16 = jnp.bfloat16
    seq_count = tokens.shape[0]
    residual = tokens.astype(f32)
    normed = rms_scale(residual, mixer_gain).astype(bf16)
    gate_pre = jnp.dot(normed, gate_weight, preferred_element_type=f32)
    inner_pre = jnp.dot(normed, inner_weight, preferred_element_type=f32).astype(bf16)
    state_pre = jnp.stack(
        [
            jnp.dot(normed, state_weight[0], preferred_element_type=f32),
            jnp.dot(normed, state_weight[1], preferred_element_type=f32),
        ],
        axis=1,
    ).astype(bf16)
    step_raw = jnp.dot(normed, step_weight, preferred_element_type=f32)
    inner_ctx = jnp.concatenate([inner_window, inner_pre[:, None, :]], axis=1)
    inner_conv = jax.nn.silu(jnp.sum(inner_ctx.astype(f32) * inner_kernel[None], axis=1))
    state_ctx = jnp.concatenate([state_window, state_pre[:, None]], axis=1)
    state_conv = jax.nn.silu(jnp.sum(state_ctx.astype(f32) * state_kernel[None], axis=1))
    per_group = HEADS // GROUPS
    local_groups = state_conv.shape[-1] // STATE_DIM
    step_size = jax.nn.softplus(step_raw + step_bias)
    decay_rate = jnp.exp(-step_size * jnp.exp(decay_log))
    shaped = (seq_count, local_groups, per_group)
    inner_heads = inner_conv.reshape(seq_count, local_groups, per_group, HEAD_DIM)
    in_vector = state_conv[:, 0].reshape(seq_count, local_groups, STATE_DIM)
    out_vector = state_conv[:, 1].reshape(seq_count, local_groups, STATE_DIM)
    old_state = recurrent_state.reshape(seq_count, local_groups, per_group, HEAD_DIM, STATE_DIM)
    written = (step_size.reshape(shaped)[..., None] * inner_heads)[..., None] * in_vector[
        :, :, None, None, :
    ]
    new_state = old_state * decay_rate.reshape(shaped)[..., None, None] + written
    mixed_out = jnp.sum(new_state * out_vector[:, :, None, None, :], axis=-1)
    mixed_out = (
        mixed_out + skip_scale.reshape(local_groups, per_group)[None, :, :, None] * inner_heads
    )
    gated_out = mixed_out.reshape(seq_count, -1) * jax.nn.silu(gate_pre)
    grouped = rms_scale(gated_out.reshape(seq_count, local_groups, -1), 1.0).reshape(seq_count, -1)
    mixer_rows = (grouped * group_gain).astype(bf16)
    partial_value = jnp.dot(mixer_rows, output_weight, preferred_element_type=f32).astype(bf16)
    ep_size = lax.axis_size("ep")
    tp_size = lax.axis_size("tp")
    width = tokens.shape[1]
    own_width = width // tp_size
    total = ep_size * seq_count
    block = total // tp_size
    hidden_width = dense_gate.shape[1]
    lanes = -(-ep_size // 128) * 128
    mix = jnp.sum(
        jnp.where(
            routes[:, :, None] == jnp.arange(lanes, dtype=jnp.int32)[None, None, :],
            route_weights[:, :, None],
            0.0,
        ),
        axis=1,
    )
    vmem = pl.BlockSpec(memory_space=pltpu.VMEM)
    hbm = pl.BlockSpec(memory_space=pl.ANY)
    dma = pltpu.SemaphoreType.DMA
    new_tokens = pl.pallas_call(
        functools.partial(branches, ep_size, tp_size),
        out_shape=jax.ShapeDtypeStruct((seq_count, own_width), bf16),
        in_specs=[vmem] * 5 + [hbm] * 6,
        out_specs=vmem,
        scratch_shapes=[
            pltpu.VMEM(expert_gate.shape, bf16),
            pltpu.VMEM(expert_up.shape, bf16),
            pltpu.VMEM(expert_down.shape, bf16),
            pltpu.VMEM(dense_gate.shape, bf16),
            pltpu.VMEM(dense_up.shape, bf16),
            pltpu.VMEM(dense_down.shape, bf16),
            pltpu.VMEM((tp_size, seq_count, width), bf16),
            pltpu.VMEM((ep_size, seq_count, lanes), f32),
            pltpu.VMEM((seq_count, width), f32),
            pltpu.VMEM((2, ep_size, seq_count, width // 2), bf16),
            pltpu.VMEM((total, width), f32),
            pltpu.VMEM((total, width), bf16),
            pltpu.VMEM((tp_size, 2, block, hidden_width), bf16),
            pltpu.VMEM((tp_size, 2, block, hidden_width), bf16),
            pltpu.VMEM((tp_size, block, hidden_width), bf16),
            pltpu.VMEM((tp_size, total, own_width), bf16),
            pltpu.VMEM((tp_size, total, own_width), bf16),
            pltpu.VMEM((ep_size, seq_count, own_width), bf16),
            pltpu.VMEM((ep_size, seq_count, own_width), bf16),
            dma((6,)),
            dma((2, tp_size)),
            dma((2, ep_size)),
            dma((2, ep_size)),
            dma((2, ep_size)),
            dma((2, tp_size)),
            dma((2, tp_size)),
            dma((2, tp_size)),
            dma((2, ep_size)),
        ],
        compiler_params=pltpu.CompilerParams(
            collective_id=0, has_side_effects=True, vmem_limit_bytes=60 * 1024 * 1024
        ),
    )(
        partial_value,
        tokens,
        channel_gain[None],
        mix,
        dense_scale[None],
        expert_gate,
        expert_up,
        expert_down,
        dense_gate,
        dense_up,
        dense_down,
    )
    return (
        new_tokens,
        new_state.reshape(seq_count, -1, HEAD_DIM, STATE_DIM),
        inner_ctx[:, 1:],
        state_ctx[:, 1:],
    )


def solution(mesh):
    placed = (
        P("ep", None),
        P(),
        P(None, "tp"),
        P(None, "tp"),
        P(None, None, "tp"),
        P(None, "tp"),
        P("tp"),
        P("tp"),
        P("tp"),
        P(None, "tp"),
        P(None, None, "tp"),
        P("ep", None, "tp"),
        P("ep", None, None, "tp"),
        P("ep", "tp", None, None),
        P("tp"),
        P("tp", None),
        P(),
        P("ep", None),
        P("ep", None),
        P("ep", None, "tp"),
        P("ep", None, "tp"),
        P("ep", "tp", None),
        P("tp", "ep"),
        P("tp", "ep"),
        P("ep", "tp"),
        P("tp"),
    )
    return jax.shard_map(
        local,
        mesh=mesh,
        in_specs=placed,
        out_specs=(
            P("ep", "tp"),
            P("ep", "tp", None, None),
            P("ep", None, "tp"),
            P("ep", None, None, "tp"),
        ),
        check_vma=False,
    )
```

time: 160 us -> 65.3 us (0.41); the launches traced: 157 us -> 64.7 us
  waiting for transfers between devices: 83.9 us -> 0 us
  Pallas kernels: 0 us -> 36 us
  matrix products: 24.6 us -> 7.67 us
  between operations: 15.6 us -> 0.76 us
  blocking collectives: 11.8 us -> 0 us
  starting transfers between devices: 9.28 us -> 0 us
  local copies, waits for them, and re-layouts: 4.14 us -> 11.2 us
    all_gather x3 -> x0, waiting for transfers between devices: 46.6 us -> none  [the longest x1 33.5 us: local(): lax.all_gather(dense_up, 'ep', axis=1, tiled=True)]
    pallas_call x0 -> x1, Pallas kernels: none -> 36 us  [local(): pl.pallas_call(functools.partial(branches, ep_size, tp_size), out_shape=j...]
    psum x1 -> x0, waiting for transfers between devices: 19.5 us -> none  [local(): gate_up = lax.psum(gate_up.astype(jnp.bfloat16), 'tp').astype(jnp.float32)]
    dot_general x9 -> x1, matrix products: 19.6 us -> 1.52 us  [local(): jnp.dot(mixer_rows, output_weight, preferred_element_type=f32).astype(bf16)]
    all_to_all x2 -> x0, waiting for transfers between devices: 15.8 us -> none  [the longest x1 10.6 us: local(): lax.all_to_all(outgoing, 'ep', split_axis=0, concat_axis=0, tiled=True)]
    psum x1 -> x0, blocking collectives: 11.8 us -> none  [local(): lax.psum(partial_value.astype(jnp.bfloat16), 'tp').astype(jnp.float32)]
    all_to_all x2 -> x0, starting transfers between devices: 9.08 us -> none  [the longest x1 5.72 us: local(): lax.all_to_all(outgoing, 'ep', split_axis=0, concat_axis=0, tiled=True)]
    unnamed x48 -> x28, local copies, waits for them, and re-layouts: 0.67 us -> 7.86 us
  transfers between devices with their start and end apart: 7 -> 0, of which waited for: 5 -> 0; matrix products, arithmetic and copies ran while one was open for 22% -> 0% of each run, Pallas kernels for 0% -> 0%
where the time goes in v1:
time: 65.3 us; the launch traced here: 64.7 us
  Pallas kernels  36 us (55%)
  local copies, waits for them, and re-layouts  11.2 us (17%)
  other arithmetic  9.03 us (14%)
  matrix products  7.67 us (12%)
  between operations  0.76 us (1%)
    pallas_call x1, Pallas kernels, local(): pl.pallas_call(functools.partial(branches, ep_size, tp_size), out_shape=j...  36 us
    unnamed x28, local copies, waits for them, and re-layouts  7.86 us
    reduce_sum x1, other arithmetic, local(): mixed_out = jnp.sum(new_state * out_vector[:, :, None, None, :], axis=-1)  5.03 us
    reduce_sum x1, local copies, waits for them, and re-layouts, local(): mixed_out = jnp.sum(new_state * out_vector[:, :, None, None, :], axis=-1)  1.61 us
    dot_general x1, matrix products, local(): jnp.dot(mixer_rows, output_weight, preferred_element_type=f32).astype(bf16)  1.52 us
    dot_general x1, matrix products, local(): gate_pre = jnp.dot(normed, gate_weight, preferred_element_type=f32)  1.39 us
    dot_general x1, matrix products, local(): jnp.dot(normed, inner_weight, preferred_element_type=f32).astype(bf16)  1.31 us

profile of v1, /device:TPU:1, one launch (start us, length us, event | category | flops | bytes accessed | tf_op | source)
XLA Modules:
  0.0 64.7 jit_solution(17843816602449560965)
XLA Ops:
  0.6 0.0 copy-start
  0.6 1.0 %fusion.7 = f32[24]{0:T(128)S(1)} fusion(bf16[24,1024]{1,0:T(8,128)(2,1)} %tokens.1), kind=kLoop, calls=%fused_computation.16 | loop fusion | flops 73704 | bytes 49248 | tf_op jit(solution)/shard_map/reduce_sum | solution.py:20
  1.6 0.0 copy-start.7
  1.6 1.3 %fusion = bf16[24,1,256]{2,0,1:T(8,128)(2,1)S(1)} fusion(bf16[1024,256]{1,0:T(8,128)(2,1)} %param.29, bf16[24,1024]{1,0:T(8,128)(2,1)} %tokens.1, f32[1024]{0:T(1024)} %param.27, f32[24]{0:T(128)S(1)} %add_rsqrt_fusion.1), kind=kOutput, calls=%fused_computation.4 | convolution fusion | flops 12687360 | bytes 589920 | tf_op jit(solution)/shard_map/dot_general | solution.py:305
  3.0 0.8 %multiply_reduce_fusion.2 = f32[24,256]{1,0:T(8,128)S(1)} fusion(bf16[24,1,256]{2,0,1:T(8,128)(2,1)S(1)} %fusion, bf16[24,3,256]{2,0,1:T(8,128)(2,1)} %param.37, f32[4,256]{1,0:T(4,128)} %param.35), kind=kLoop, calls=%fused_computation.20 | loop fusion | flops 92160 | bytes 77824 | tf_op jit(solution)/shard_map/reduce_sum | solution.py:315
  3.8 0.1 reduce_sum.60
  3.8 0.7 %exp.33 = f32[4]{0:T(128)S(1)} exponential(f32[4]{0:T(128)} %param.33) | non-fusion elementwise | bytes 32 | tf_op jit(solution)/shard_map/exp | solution.py:321
  4.5 1.0 %multiply_exponential_fusion = (f32[24,4]{0,1:T(4,128)S(1)}, f32[24,4]{0,1:T(4,128)S(1)}) fusion(f32[4]{0:T(128)S(1)} %exp.33, f32[4]{0:T(128)} %param.32, bf16[1024,4]{0,1:T(4,128)(2,1)} %param.31, bf16[24,1024]{1,0:T(8,128)(2,1)} %tokens.1, f32[1024]{0:T(1024)} %param.27, f32[24]{0:T(128)S(1)} %add_rsqrt_fusion.1), kind=kOutput, calls=%fused_computation.39 | convolution fusion | flops 295776 | bytes 62336 | tf_op jit(solution)/shard_map/dot_general | solution.py:313
  5.5 0.1 copy.49
  5.6 0.1 fusion.10
  5.7 1.2 %fusion.1 = bf16[24,1,1,128]{3,0,2,1:T(8,128)(2,1)S(1)} fusion(bf16[2,1024,128]{2,1,0:T(8,128)(2,1)} %param.30, bf16[24,1024]{1,0:T(8,128)(2,1)} %tokens.1, f32[1024]{0:T(1024)} %param.27, f32[24]{0:T(128)S(1)} %add_rsqrt_fusion.1), kind=kOutput, calls=%fused_computation.7 | convolution fusion | flops 6392832 | bytes 321632 | tf_op jit(solution)/shard_map/dot_general | solution.py:308
  6.9 0.0 copy-done.7
  7.0 1.2 %fusion.2 = bf16[24,1,1,128]{3,0,2,1:T(8,128)(2,1)S(1)} fusion(bf16[2,1024,128]{2,1,0:T(8,128)(2,1)} %param.30, bf16[24,1024]{1,0:T(8,128)(2,1)} %tokens.1, f32[1024]{0:T(1024)} %param.27, f32[24]{0:T(128)S(1)} %add_rsqrt_fusion.1), kind=kOutput, calls=%fused_computation.8 | convolution fusion | flops 6392832 | bytes 321632 | tf_op jit(solution)/shard_map/dot_general | solution.py:309
  8.2 0.8 %constant_dynamic-update-slice_fusion = bf16[24,4,2,128]{3,2,1,0:T(2,128)(2,1)S(1)} fusion(bf16[24,3,2,128]{3,2,1,0:T(2,128)(2,1)} %param.38), kind=kLoop, calls=%fused_computation.37 | loop fusion | bytes 73728
  9.0 0.8 %multiply_reduce_fusion.1 = f32[24,2,128]{2,1,0:T(2,128)S(1)} fusion(bf16[24,4,2,128]{3,2,1,0:T(2,128)(2,1)S(1)} %copy_dynamic-update-slice_fusion, f32[4,2,128]{2,1,0:T(2,128)} %param.36), kind=kLoop, calls=%fused_computation.19 | loop fusion | flops 67584 | bytes 77824 | tf_op jit(solution)/shard_map/reduce_sum | solution.py:317
  9.8 0.1 copy.48
  9.9 0.0 copy-start.10
  9.9 0.0 copy-start.3
  9.9 0.0 copy-start.6
  9.9 5.0 %multiply_reduce_fusion = (f32[24,4,64]{2,1,0:T(4,128)}, f32[24,4,64,128]{3,2,1,0:T(8,128)}) fusion(f32[24,128]{1,0:T(8,128)S(1)} %bitcast.21, f32[24,128]{1,0:T(8,128)S(1)} %bitcast.20, f32[24,4,64]{2,1,0:T(4,128)S(1)} %fusion.10, f32[24,4,64,128]{3,2,1,0:T(8,128)} %param.39, f32[24,4]{1,0:T(8,128)S(1)} %copy.48), kind=kLoop, calls=%fused_computation | loop fusion | flops 3926016 | bytes 6365568 | tf_op jit(solution)/shard_map/reduce_sum | solution.py:331
  15.0 0.0 copy-start.2
  15.0 1.6 %reduce_sum.63 = f32[24,256]{1,0:T(8,128)} reshape(f32[24,4,64]{2,1,0:T(4,128)} %get-tuple-element.4) | data formatting | bytes 49152 | tf_op jit(solution)/shard_map/reduce_sum | solution.py:331
  16.6 0.0 copy-done.10
  16.6 0.1 mul.178
  16.7 0.1 mul.179
  16.7 0.0 copy-done.3
  16.7 0.0 copy-done.6
  16.8 1.4 %multiply_reduce_fusion.3 = (f32[24]{0:T(128)S(1)}, f32[24,256]{1,0:T(8,128)S(1)}) fusion(bf16[1024,256]{1,0:T(8,128)(2,1)} %param.28, bf16[24,1024]{1,0:T(8,128)(2,1)S(1)} %copy-done.3, f32[1024]{0:T(1024)S(1)} %copy-done.6, f32[24]{0:T(128)} %copy-done.7, f32[24,256]{1,0:T(8,128)} %reduce_sum.63, f32[24,256]{1,0:T(8,128)S(1)} %multiply_reduce_fusion.2, ...), kind=kOutput, calls=%fused_computation.31 | convolution fusion | flops 12761064 | bytes 652480 | tf_op jit(solution)/shard_map/dot_general | solution.py:304
  18.2 0.0 copy-done
  18.2 1.5 %convolution_convert_fusion.part = bf16[24,1024]{1,0:T(8,128)(2,1)} fusion(bf16[256,1024]{1,0:T(8,128)(2,1)S(1)} %copy-done, f32[24,256]{1,0:T(8,128)S(1)} %get-tuple-element.11, f32[256]{0:T(256)} %param.40, f32[24]{0:T(128)S(1)} %add_rsqrt_fusion), kind=kOutput, calls=%fused_computation.2 | convolution fusion | flops 12625920 | bytes 599136 | tf_op jit(solution)/shard_map/dot_general | solution.py:338
  19.7 0.0 copy-done.1
  19.7 0.0 copy-start.8
  19.7 0.0 copy-start.9
  19.7 1.6 %copy.51.gate_hbm = bf16[1,1024,704]{2,1,0:T(8,128)(2,1)} copy(bf16[1,1024,704]{1,2,0:T(8,128)(2,1)S(1)} %copy-done.1) | data formatting | bytes 2883584 | tf_op args[19]
  21.3 0.0 copy-done.2
  21.3 0.0 copy-start.4
  21.3 1.6 %copy.52.up_hbm = bf16[1,1024,704]{2,1,0:T(8,128)(2,1)} copy(bf16[1,1024,704]{1,2,0:T(8,128)(2,1)S(1)} %copy-done.2) | data formatting | bytes 2883584 | tf_op args[20]
  22.9 1.7 %copy.53.dgate_hbm = bf16[256,352]{1,0:T(8,128)(2,1)} copy(bf16[256,352]{0,1:T(8,128)(2,1)} %param.48) | data formatting | bytes 360448 | tf_op args[22]
  24.6 0.0 copy-done.4
  24.6 0.8 %copy.54.dup_hbm = bf16[256,352]{1,0:T(8,128)(2,1)} copy(bf16[256,352]{0,1:T(8,128)(2,1)S(1)} %copy-done.4) | data formatting | bytes 360448 | tf_op args[23]
  25.4 0.0 copy-done.8
  25.4 0.0 copy-done.9
  25.4 0.7 %select_reduce_fusion.mix = f32[24,128]{1,0:T(8,128)} fusion(f32[24,2]{0,1:T(2,128)S(1)} %copy-done.8, s32[24,2]{0,1:T(2,128)S(1)} %copy-done.9), kind=kLoop, calls=%fused_computation.28 | loop fusion | flops 15360 | bytes 12672 | tf_op jit(solution)/shard_map/reduce_sum | solution.py:347
  26.1 36.0 %shard_map.273 = bf16[24,256]{1,0:T(8,128)(2,1)} custom-call(bf16[24,1024]{1,0:T(8,128)(2,1)} %convolution_convert_fusion.part, bf16[24,1024]{1,0:T(8,128)(2,1)} %tokens.1, f32[1,1024]{1,0:T(1,128)} %bitcast.22, f32[24,128]{1,0:T(8,128)} %select_reduce_fusion.mix, f32[1,256]{1,0:T(1,128)} %bitcast.23, bf16[1,1024,704]{2,1,0:T(8,128)(2,1)} %copy.51.gate_hbm, ...), custom_call_target="tpu_custom_call" | custom-call | tf_op jit(solution)/shard_map/pallas_call | solution.py:358
  62.1 0.6 slice.28
  62.7 0.0 copy-done.5
  62.7 0.6 fusion.11
  63.3 1.3 %copy.58 = bf16[24,256]{1,0:T(8,128)(2,1)} copy(bf16[24,256]{1,0:T(8,128)(2,1)} %shard_map.273) | data formatting | bytes 24576
  (8 shorter events, 0.1 us)
Async XLA Ops:
  0.6 17.5 %copy-start = (bf16[256,1024]{1,0:T(8,128)(2,1)S(1)}, bf16[256,1024]{1,0:T(8,128)(2,1)}, u32[]{:S(2)}) copy-start(bf16[256,1024]{1,0:T(8,128)(2,1)} %param.41) | copy-start | bytes 1572868
  1.6 5.3 %copy-start.7 = (f32[24]{0:T(128)}, f32[24]{0:T(128)S(1)}, u32[]{:S(2)}) copy-start(f32[24]{0:T(128)S(1)} %add_rsqrt_fusion.1) | copy-start | bytes 292
  9.9 6.7 %copy-start.10 = (f32[4]{0:T(128)S(1)}, f32[4]{0:T(128)}, u32[]{:S(2)}) copy-start(f32[4]{0:T(128)} %param.34) | copy-start | bytes 52
  9.9 6.8 %copy-start.3 = (bf16[24,1024]{1,0:T(8,128)(2,1)S(1)}, bf16[24,1024]{1,0:T(8,128)(2,1)}, u32[]{:S(2)}) copy-start(bf16[24,1024]{1,0:T(8,128)(2,1)} %tokens.1) | copy-start | bytes 147460
  9.9 6.8 %copy-start.6 = (f32[1024]{0:T(1024)S(1)}, f32[1024]{0:T(1024)}, u32[]{:S(2)}) copy-start(f32[1024]{0:T(1024)} %param.27) | copy-start | bytes 12292
  9.9 9.8 %copy-start.1 = (bf16[1,1024,704]{1,2,0:T(8,128)(2,1)S(1)}, bf16[1,1024,704]{1,2,0:T(8,128)(2,1)}, u32[]{:S(2)}) copy-start(bf16[1,1024,704]{1,2,0:T(8,128)(2,1)} %param.45) | copy-start | bytes 4325380
  15.0 6.3 %copy-start.2 = (bf16[1,1024,704]{1,2,0:T(8,128)(2,1)S(1)}, bf16[1,1024,704]{1,2,0:T(8,128)(2,1)}, u32[]{:S(2)}) copy-start(bf16[1,1024,704]{1,2,0:T(8,128)(2,1)} %param.46) | copy-start | bytes 4325380
  19.7 5.7 %copy-start.8 = (f32[24,2]{0,1:T(2,128)S(1)}, f32[24,2]{0,1:T(2,128)}, u32[]{:S(2)}) copy-start(f32[24,2]{0,1:T(2,128)} %param.44) | copy-start | bytes 580
  19.7 5.7 %copy-start.9 = (s32[24,2]{0,1:T(2,128)S(1)}, s32[24,2]{0,1:T(2,128)}, u32[]{:S(2)}) copy-start(s32[24,2]{0,1:T(2,128)} %param.43) | copy-start | bytes 580
  21.3 3.3 %copy-start.4 = (bf16[256,352]{0,1:T(8,128)(2,1)S(1)}, bf16[256,352]{0,1:T(8,128)(2,1)}, u32[]{:S(2)}) copy-start(bf16[256,352]{0,1:T(8,128)(2,1)} %param.49) | copy-start | bytes 540676
  22.9 39.9 %copy-start.5 = (bf16[24,3,256]{2,0,1:T(8,128)(2,1)S(1)}, bf16[24,3,256]{2,0,1:T(8,128)(2,1)}, u32[]{:S(2)}) copy-start(bf16[24,3,256]{2,0,1:T(8,128)(2,1)} %param.37) | copy-start | bytes 110596

commit v2 on v1

--- a/solution.py
+++ b/solution.py
@@ -23,6 +23,12 @@
 
 def silu(v):
     return v / (1.0 + jnp.exp(-v))
+
+
+def dot_rows(rows, columns):
+    return lax.dot_general(
+        rows, columns, (((1,), (1,)), ((), ())), preferred_element_type=jnp.float32
+    )
 
 
 def branches(
@@ -167,8 +173,8 @@
     own = pl.ds(pl.multiple_of(me_t * own_width, own_width), own_width)
     for t in range(tp_size):
         piece = packed[t * block : (t + 1) * block, own]
-        pre_send[t, 0] = jnp.dot(piece, dgate_w[...], preferred_element_type=f32).astype(bf16)
-        pre_send[t, 1] = jnp.dot(piece, dup_w[...], preferred_element_type=f32).astype(bf16)
+        pre_send[t, 0] = dot_rows(piece, dgate_w[...]).astype(bf16)
+        pre_send[t, 1] = dot_rows(piece, dup_w[...]).astype(bf16)
     pre_copies = [
         remote(pre_send.at[tp_peers[d]], pre_recv.at[d], pre_sems, d, me_e, tp_peers[d])
         for d in range(1, tp_size)
@@ -189,8 +195,8 @@
     def experts(step, carry):
         at = pl.ds(pl.multiple_of(step * chunk, chunk), chunk)
         x = packed[at, :]
-        gate_act = jnp.dot(x, gate_w[0], preferred_element_type=f32)
-        up_act = jnp.dot(x, up_w[0], preferred_element_type=f32)
+        gate_act = dot_rows(x, gate_w[0])
+        up_act = dot_rows(x, up_w[0])
         activated = (silu(gate_act) * up_act).astype(bf16)
         weights = mixes[pl.ds(step * chunk_blocks, chunk_blocks)].reshape(chunk, mix.shape[1])
         lanes = lax.broadcasted_iota(jnp.int32, weights.shape, 1)
@@ -343,6 +349,10 @@
     total = ep_size * seq_count
     block = total // tp_size
     hidden_width = dense_gate.shape[1]
+    expert_gate = jnp.swapaxes(expert_gate, 1, 2)
+    expert_up = jnp.swapaxes(expert_up, 1, 2)
+    dense_gate = dense_gate.T
+    dense_up = dense_up.T
     lanes = -(-ep_size // 128) * 128
     mix = jnp.sum(
         jnp.where(

time: 65.3 us -> 55.8 us (0.85)
  local copies, waits for them, and re-layouts: 11.2 us -> 4.01 us
  matrix products: 7.67 us -> 5.97 us
  other arithmetic: 9.03 us -> 8.35 us
    unnamed x28 -> x20, local copies, waits for them, and re-layouts: 7.86 us -> 2.15 us
    reduce_sum x1, local copies, waits for them, and re-layouts: 1.61 us -> 0.1 us  [local(): mixed_out = jnp.sum(new_state * out_vector[:, :, None, None, :], axis=-1)]
    dot_general x1, matrix products: 1.39 us -> 0.35 us  [local(): gate_pre = jnp.dot(normed, gate_weight, preferred_element_type=f32)]
    reduce_sum x1, other arithmetic: 5.03 us -> 4.36 us  [local(): mixed_out = jnp.sum(new_state * out_vector[:, :, None, None, :], axis=-1)]
    dot_general x1, matrix products: 1.52 us -> 0.85 us  [local(): jnp.dot(mixer_rows, output_weight, preferred_element_type=f32).astype(bf16)]
where the time goes in v2:
time: 55.8 us; the launch traced here: 55.2 us
  Pallas kernels  36.1 us (65%)
  other arithmetic  8.35 us (15%)
  matrix products  5.97 us (11%)
  local copies, waits for them, and re-layouts  4.01 us (7%)
  between operations  0.78 us (1%)
    pallas_call x1, Pallas kernels, local(): pl.pallas_call(functools.partial(branches, ep_size, tp_size), out_shape=j...  36.1 us
    reduce_sum x1, other arithmetic, local(): mixed_out = jnp.sum(new_state * out_vector[:, :, None, None, :], axis=-1)  4.36 us
    unnamed x20, local copies, waits for them, and re-layouts  2.15 us
    dot_general x1, matrix products, local(): jnp.dot(normed, inner_weight, preferred_element_type=f32).astype(bf16)  1.32 us
    dot_general x1, matrix products, local(): jnp.dot(normed, state_weight[1], preferred_element_type=f32)  1.21 us
    dot_general x1, matrix products, local(): jnp.dot(normed, state_weight[0], preferred_element_type=f32)  1.2 us

profile of v2, /device:TPU:1, one launch (start us, length us, event | category | flops | bytes accessed | tf_op | source)
XLA Modules:
  0.0 55.2 jit_solution(4496111890614216864)
XLA Ops:
  0.6 0.0 copy-start
  0.6 1.0 %fusion.7 = f32[24]{0:T(128)S(1)} fusion(bf16[24,1024]{1,0:T(8,128)(2,1)} %tokens.1), kind=kLoop, calls=%fused_computation.16 | loop fusion | flops 73704 | bytes 49248 | tf_op jit(solution)/shard_map/reduce_sum | solution.py:20
  1.6 1.3 %fusion = bf16[24,1,256]{2,0,1:T(8,128)(2,1)S(1)} fusion(bf16[1024,256]{1,0:T(8,128)(2,1)} %param.29, bf16[24,1024]{1,0:T(8,128)(2,1)} %tokens.1, f32[1024]{0:T(1024)} %param.27, f32[24]{0:T(128)S(1)} %add_rsqrt_fusion.1), kind=kOutput, calls=%fused_computation.4 | convolution fusion | flops 12687360 | bytes 589920 | tf_op jit(solution)/shard_map/dot_general | solution.py:311
  2.9 0.8 %multiply_reduce_fusion.2 = f32[24,256]{1,0:T(8,128)S(1)} fusion(bf16[24,1,256]{2,0,1:T(8,128)(2,1)S(1)} %fusion, bf16[24,3,256]{2,0,1:T(8,128)(2,1)} %param.37, f32[4,256]{1,0:T(4,128)} %param.35), kind=kLoop, calls=%fused_computation.20 | loop fusion | flops 92160 | bytes 77824 | tf_op jit(solution)/shard_map/reduce_sum | solution.py:321
  3.7 0.1 reduce_sum.60
  3.8 0.7 %exp.33 = f32[4]{0:T(128)S(1)} exponential(f32[4]{0:T(128)} %param.33) | non-fusion elementwise | bytes 32 | tf_op jit(solution)/shard_map/exp | solution.py:327
  4.5 1.0 %multiply_exponential_fusion = (f32[24,4]{0,1:T(4,128)S(1)}, f32[24,4]{0,1:T(4,128)S(1)}) fusion(f32[4]{0:T(128)S(1)} %exp.33, f32[4]{0:T(128)} %param.32, bf16[1024,4]{0,1:T(4,128)(2,1)} %param.31, bf16[24,1024]{1,0:T(8,128)(2,1)} %tokens.1, f32[1024]{0:T(1024)} %param.27, f32[24]{0:T(128)S(1)} %add_rsqrt_fusion.1), kind=kOutput, calls=%fused_computation.39 | convolution fusion | flops 295776 | bytes 62336 | tf_op jit(solution)/shard_map/dot_general | solution.py:319
  5.5 0.1 copy.41
  5.6 0.1 fusion.10
  5.7 1.2 %fusion.1 = bf16[24,1,1,128]{3,0,2,1:T(8,128)(2,1)S(1)} fusion(bf16[2,1024,128]{2,1,0:T(8,128)(2,1)} %param.30, bf16[24,1024]{1,0:T(8,128)(2,1)} %tokens.1, f32[1024]{0:T(1024)} %param.27, f32[24]{0:T(128)S(1)} %add_rsqrt_fusion.1), kind=kOutput, calls=%fused_computation.7 | convolution fusion | flops 6392832 | bytes 321632 | tf_op jit(solution)/shard_map/dot_general | solution.py:314
  6.9 1.2 %fusion.2 = bf16[24,1,1,128]{3,0,2,1:T(8,128)(2,1)S(1)} fusion(bf16[2,1024,128]{2,1,0:T(8,128)(2,1)} %param.30, bf16[24,1024]{1,0:T(8,128)(2,1)} %tokens.1, f32[1024]{0:T(1024)} %param.27, f32[24]{0:T(128)S(1)} %add_rsqrt_fusion.1), kind=kOutput, calls=%fused_computation.8 | convolution fusion | flops 6392832 | bytes 321632 | tf_op jit(solution)/shard_map/dot_general | solution.py:315
  8.2 0.8 %constant_dynamic-update-slice_fusion = bf16[24,4,2,128]{3,2,1,0:T(2,128)(2,1)S(1)} fusion(bf16[24,3,2,128]{3,2,1,0:T(2,128)(2,1)} %param.38), kind=kLoop, calls=%fused_computation.37 | loop fusion | bytes 73728
  9.0 0.8 %multiply_reduce_fusion.1 = f32[24,2,128]{2,1,0:T(2,128)S(1)} fusion(bf16[24,4,2,128]{3,2,1,0:T(2,128)(2,1)S(1)} %copy_dynamic-update-slice_fusion, f32[4,2,128]{2,1,0:T(2,128)} %param.36), kind=kLoop, calls=%fused_computation.19 | loop fusion | flops 67584 | bytes 77824 | tf_op jit(solution)/shard_map/reduce_sum | solution.py:323
  9.8 0.1 copy.40
  9.9 0.0 copy-start.8
  9.9 0.0 copy-start.1
  9.9 0.0 copy-start.2
  9.9 0.0 copy-start.4
  9.9 0.0 copy-start.5
  9.9 0.0 copy-start.6
  10.0 0.0 copy-start.7
  10.0 4.4 %multiply_reduce_fusion = (f32[24,4,64]{2,1,0:T(4,128)S(1)}, f32[24,4,64,128]{3,2,1,0:T(8,128)}) fusion(f32[24,128]{1,0:T(8,128)S(1)} %bitcast.29, f32[24,128]{1,0:T(8,128)S(1)} %bitcast.28, f32[24,4,64]{2,1,0:T(4,128)S(1)} %fusion.10, f32[24,4,64,128]{3,2,1,0:T(8,128)} %param.39, f32[24,4]{1,0:T(8,128)S(1)} %copy.40), kind=kLoop, calls=%fused_computation | loop fusion | flops 3926016 | bytes 6365568 | tf_op jit(solution)/shard_map/reduce_sum | solution.py:337
  14.3 0.1 reduce_sum.63
  14.4 0.0 copy-done.8
  14.4 0.1 mul.178
  14.5 0.1 mul.179
  14.6 0.0 copy-done.1
  14.6 0.0 copy-done.2
  14.6 0.0 copy-done.4
  14.6 0.0 copy-start.3
  14.6 0.4 multiply_reduce_fusion.3
  15.0 0.0 copy-done
  15.0 0.0 copy-done.5
  15.0 0.8 %convolution_convert_fusion.part = bf16[24,1024]{1,0:T(8,128)(2,1)} fusion(bf16[256,1024]{1,0:T(8,128)(2,1)S(1)} %copy-done, f32[24,256]{1,0:T(8,128)S(1)} %get-tuple-element.11, f32[256]{0:T(256)S(1)} %copy-done.5, f32[24]{0:T(128)S(1)} %add_rsqrt_fusion), kind=kOutput, calls=%fused_computation.2 | convolution fusion | flops 12625920 | bytes 599136 | tf_op jit(solution)/shard_map/dot_general | solution.py:344
  15.8 0.0 copy-done.6
  15.8 0.0 copy-done.7
  15.8 0.7 %select_reduce_fusion.mix = f32[24,128]{1,0:T(8,128)} fusion(f32[24,2]{0,1:T(2,128)S(1)} %copy-done.6, s32[24,2]{0,1:T(2,128)S(1)} %copy-done.7), kind=kLoop, calls=%fused_computation.28 | loop fusion | flops 15360 | bytes 12672 | tf_op jit(solution)/shard_map/reduce_sum | solution.py:357
  16.5 36.1 %shard_map.273 = bf16[24,256]{1,0:T(8,128)(2,1)} custom-call(bf16[24,1024]{1,0:T(8,128)(2,1)} %convolution_convert_fusion.part, bf16[24,1024]{1,0:T(8,128)(2,1)} %tokens.1, f32[1,1024]{1,0:T(1,128)} %bitcast.30, f32[24,128]{1,0:T(8,128)} %select_reduce_fusion.mix, f32[1,256]{1,0:T(1,128)} %bitcast.31, bf16[1,704,1024]{2,1,0:T(8,128)(2,1)} %bitcast.24, ...), custom_call_target="tpu_custom_call" | custom-call | tf_op jit(solution)/shard_map/pallas_call | solution.py:368
  52.7 0.6 %slice.28 = bf16[24,3,2,128]{3,2,1,0:T(2,128)(2,1)} slice(bf16[24,4,2,128]{3,2,1,0:T(2,128)(2,1)S(1)} %copy_dynamic-update-slice_fusion), slice={[0:24], [1:4], [0:2], [0:128]} | slice | bytes 73728 | tf_op jit(solution)/shard_map/slice | solution.py:423
  53.3 0.0 copy-done.3
  53.3 0.6 %fusion.11 = bf16[24,3,256]{2,0,1:T(8,128)(2,1)} fusion(bf16[24,3,256]{2,0,1:T(8,128)(2,1)S(1)} %copy-done.3, bf16[24,1,256]{2,0,1:T(8,128)(2,1)S(1)} %fusion), kind=kLoop, calls=%fused_computation.26 | loop fusion | flops 18432 | bytes 86016 | tf_op jit(solution)/shard_map/concatenate | solution.py:320
  53.9 1.3 %copy.46 = bf16[24,256]{1,0:T(8,128)(2,1)} copy(bf16[24,256]{1,0:T(8,128)(2,1)} %shard_map.273) | data formatting | bytes 24576
  (6 shorter events, 0.1 us)
Async XLA Ops:
  0.6 14.3 %copy-start = (bf16[256,1024]{1,0:T(8,128)(2,1)S(1)}, bf16[256,1024]{1,0:T(8,128)(2,1)}, u32[]{:S(2)}) copy-start(bf16[256,1024]{1,0:T(8,128)(2,1)} %param.41) | copy-start | bytes 1572868
  9.9 4.5 %copy-start.8 = (f32[4]{0:T(128)S(1)}, f32[4]{0:T(128)}, u32[]{:S(2)}) copy-start(f32[4]{0:T(128)} %param.34) | copy-start | bytes 52
  9.9 4.7 %copy-start.1 = (bf16[24,1024]{1,0:T(8,128)(2,1)S(1)}, bf16[24,1024]{1,0:T(8,128)(2,1)}, u32[]{:S(2)}) copy-start(bf16[24,1024]{1,0:T(8,128)(2,1)} %tokens.1) | copy-start | bytes 147460
  9.9 4.7 %copy-start.2 = (bf16[1024,256]{1,0:T(8,128)(2,1)S(1)}, bf16[1024,256]{1,0:T(8,128)(2,1)}, u32[]{:S(2)}) copy-start(bf16[1024,256]{1,0:T(8,128)(2,1)} %param.28) | copy-start | bytes 1572868
  9.9 4.7 %copy-start.4 = (f32[1024]{0:T(1024)S(1)}, f32[1024]{0:T(1024)}, u32[]{:S(2)}) copy-start(f32[1024]{0:T(1024)} %param.27) | copy-start | bytes 12292
  9.9 5.0 %copy-start.5 = (f32[256]{0:T(256)S(1)}, f32[256]{0:T(256)}, u32[]{:S(2)}) copy-start(f32[256]{0:T(256)} %param.40) | copy-start | bytes 3076
  9.9 5.9 %copy-start.6 = (f32[24,2]{0,1:T(2,128)S(1)}, f32[24,2]{0,1:T(2,128)}, u32[]{:S(2)}) copy-start(f32[24,2]{0,1:T(2,128)} %param.44) | copy-start | bytes 580
  10.0 5.9 %copy-start.7 = (s32[24,2]{0,1:T(2,128)S(1)}, s32[24,2]{0,1:T(2,128)}, u32[]{:S(2)}) copy-start(s32[24,2]{0,1:T(2,128)} %param.43) | copy-start | bytes 580
  14.6 38.7 %copy-start.3 = (bf16[24,3,256]{2,0,1:T(8,128)(2,1)S(1)}, bf16[24,3,256]{2,0,1:T(8,128)(2,1)}, u32[]{:S(2)}) copy-start(bf16[24,3,256]{2,0,1:T(8,128)(2,1)} %param.37) | copy-start | bytes 110596
